TPU v7x, 32 devices: a whole 2x2x4 slice. The times are simulated.
32 devices in a mesh: grp: 2 (over y), fs: 4 (over z), tp: 4 (over x, core).
Axes of the slice: x: 2, y: 2, z: 4, core: 2. Of those that a mesh axis runs over, the one named last changes fastest.
Arguments:
- layer_input: bfloat16 [3072, 2048], P(('grp', 'fs'), 'tp'), parts along dimension 0, may hold values from -6 to 6
- first_gain: bfloat16 [1, 2048], P(None, 'tp'), may hold values from 0.099609375 to 1.8984375
- ffn_gate_w: bfloat16 [2048, 6144], P('fs', 'tp'), may hold values from -0.125 to 0.125
- ffn_up_w: bfloat16 [2048, 6144], P('fs', 'tp'), may hold values from -0.125 to 0.125
- ffn_down_w: bfloat16 [6144, 2048], P('tp', 'fs'), may hold values from -0.078125 to 0.078125
- mixer_gain: bfloat16 [1, 2048], P(None, 'tp'), may hold values from 0.099609375 to 1.8984375
- pool_in_w: bfloat16 [2048, 1024], P('fs', 'tp'), may hold values from -0.125 to 0.125
- mixer_gate_w: bfloat16 [2048, 2048], P('fs', 'tp'), may hold values from -0.125 to 0.125
- group_mix_w: bfloat16 [8, 128, 128], P('tp'), may hold values from -0.5 to 0.5
- pool_scale: float32 [1, 1024], P(None, 'tp'), may hold values from 0.1 to 1.9
- mixer_out_w: bfloat16 [1024, 2048], P('tp', 'fs'), may hold values from -0.1875 to 0.1875
- second_gain: bfloat16 [1, 2048], P(None, 'tp'), may hold values from 0.099609375 to 1.8984375
Outputs:
- layer_output: bfloat16 [3072, 2048], P(('grp', 'fs'), 'tp'), parts along dimension 0
There are 2 independent parts, one for each index of `grp`. A program takes and returns all parts, laid end to end along the dimension named above; an argument that names none is the same for every part. Nothing has to cross between parts.
All inputs are finite; a program needn't handle non-finite values.
Results may differ from a plain program's by a relative error of at most 0.015.
Values may be sent and summed in bfloat16 or wider, within the bound.
No kernel may reach another device: no remote copies, remote signals or barrier semaphores. Data moves between devices by JAX's collectives and lax.ppermute only.
A program may use at most 64 MiB of HBM per device.

v0:
```python
import jax
import jax.numpy as jnp
from jax import lax
from jax.sharding import PartitionSpec as P


def norm_rows(values, gain):
    gathered, gain_whole = (
        lax.all_gather(values, "tp", axis=1, tiled=True),
        lax.all_gather(gain, "tp", axis=1, tiled=True),
    )
    widened = gathered.astype(jnp.float32)
    scaled = (widened * gain_whole.astype(jnp.float32)).astype(jnp.bfloat16)
    factor = lax.rsqrt(jnp.mean(widened * widened, axis=1, keepdims=True) + 1e-06)
    return (scaled, factor)


def column_sums(partial_value):
    return lax.psum_scatter(
        partial_value.astype(jnp.bfloat16), "tp", scatter_dimension=1, tiled=True
    ).astype(jnp.float32)


def add_pair(scaled, pieces):
    first_sum = jnp.dot(scaled, pieces[0], preferred_element_type=jnp.float32)
    second_sum = jnp.dot(scaled, pieces[1], preferred_element_type=jnp.float32)
    return (first_sum, second_sum)


def per_device(
    layer_input,
    first_gain,
    ffn_gate_w,
    ffn_up_w,
    ffn_down_w,
    mixer_gain,
    pool_in_w,
    mixer_gate_w,
    group_mix_w,
    pool_scale,
    mixer_out_w,
    second_gain,
):
    row_count = layer_input.shape[0]

    def feed_forward(values, gain):
        scaled, factor = norm_rows(values, gain)
        gate_sum, up_sum = add_pair(
            scaled,
            (
                lax.all_gather(ffn_gate_w, "fs", axis=0, tiled=True),
                lax.all_gather(ffn_up_w, "fs", axis=0, tiled=True),
            ),
        )
        hidden = (jax.nn.silu(factor * gate_sum) * (factor * up_sum)).astype(jnp.bfloat16)
        return jnp.dot(
            hidden,
            lax.all_gather(ffn_down_w, "fs", axis=1, tiled=True),
            preferred_element_type=jnp.float32,
        )

    first = (
        layer_input.astype(jnp.float32) + 0.5 * column_sums(feed_forward(layer_input, first_gain))
    ).astype(jnp.bfloat16)
    scaled, factor = norm_rows(first, mixer_gain)
    pool_sum, gate_sum = add_pair(
        scaled,
        (
            lax.all_gather(pool_in_w, "fs", axis=0, tiled=True),
            lax.all_gather(mixer_gate_w, "fs", axis=0, tiled=True),
        ),
    )
    pool_pre = (factor * pool_sum).astype(jnp.bfloat16)
    gate_logit = factor * gate_sum
    group_count = group_mix_w.shape[0]
    group_width = group_mix_w.shape[1]
    first_group = lax.axis_index("tp") * group_count
    values = pool_pre.astype(jnp.float32).reshape(row_count, group_count, group_width)
    running = jnp.cumsum(values, axis=0)
    positions = jnp.arange(row_count, dtype=jnp.int32)
    windows = 2 ** (1 + (first_group + jnp.arange(group_count, dtype=jnp.int32)) % 4)
    chosen = jnp.zeros_like(values)
    for span in (2, 4, 8, 16):
        lagged = jnp.pad(running, ((span, 0), (0, 0), (0, 0)))[:row_count]
        counts = jnp.minimum(positions + 1, span).astype(jnp.float32)[:, None, None]
        means = (running - lagged) / counts
        chosen = jnp.where((windows == span)[None, :, None], means, chosen)
    trail = (chosen - values).astype(jnp.bfloat16)
    mixed = jnp.einsum("tgc,gcd->tgd", trail, group_mix_w, preferred_element_type=jnp.float32)
    pooled = (mixed.reshape(row_count, group_count * group_width) * pool_scale).astype(jnp.bfloat16)
    lifted = column_sums(
        jnp.dot(
            pooled,
            lax.all_gather(mixer_out_w, "fs", axis=1, tiled=True),
            preferred_element_type=jnp.float32,
        )
    )
    second = (first.astype(jnp.float32) + jax.nn.sigmoid(gate_logit) * lifted).astype(jnp.bfloat16)
    result = second.astype(jnp.float32) + 0.5 * column_sums(feed_forward(second, second_gain))
    return result.astype(jnp.bfloat16)


def solution(mesh):
    return jax.shard_map(
        per_device,
        mesh=mesh,
        in_specs=(
            P(("grp", "fs"), "tp"),
            P(None, "tp"),
            P("fs", "tp"),
            P("fs", "tp"),
            P("tp", "fs"),
            P(None, "tp"),
            P("fs", "tp"),
            P("fs", "tp"),
            P("tp", None, None),
            P(None, "tp"),
            P("tp", "fs"),
            P(None, "tp"),
        ),
        out_specs=P(("grp", "fs"), "tp"),
        check_vma=False,
    )
```

profile of v0, /device:TPU:0, one launch (start us, length us, event | category | flops | bytes accessed | tf_op | source)
XLA Modules:
  0.0 653.4 jit_solution(9304917217902213386)
XLA Ops:
  6.5 0.7 all-gather.10.cloned.1.call-update
  7.3 0.0 all-gather.12.cloned.1.call-start
  7.3 0.7 all-gather.12.cloned.1.call-update
  8.1 0.7 all-gather.14.cloned.1.call-update
  8.8 0.5 all-gather.16.cloned.1.call-update
  9.3 0.0 reduce-scatter.4.cloned.1.call-start
  9.4 6.2 all_gather.40
  15.6 15.7 %all-gather.10.cloned.1.call-done = bf16[384,2048]{1,0:T(8,128)(2,1)} async-done(((bf16[384,512]{1,0:T(8,128)(2,1)}), bf16[384,2048]{1,0:T(8,128)(2,1)}) %all-gather.10.cloned.1.call-update) | async-done | bytes 1572880 | tf_op jit(solution)/shard_map/all_gather | solution.py:9
  31.3 1.8 fusion
  33.1 115.1 %all-gather.12.cloned.1.call-done = bf16[2048,1536]{1,0:T(8,128)(2,1)} async-done(((bf16[512,1536]{1,0:T(8,128)(2,1)}), bf16[2048,1536]{1,0:T(8,128)(2,1)}) %all-gather.12.cloned.1.call-update) | async-done | bytes 6291472 | tf_op jit(solution)/shard_map/all_gather | solution.py:51
  148.2 7.4 %convolution_multiply_fusion.3 = f32[384,1536]{1,0:T(8,128)} fusion(bf16[2048,1536]{1,0:T(8,128)(2,1)} %all-gather.12.cloned.1.call-done, bf16[384,2048]{1,0:T(8,128)(2,1)} %all-gather.10.cloned.1.call-done, f32[2048]{0:T(1024)S(1)} %bitcast.38, f32[384]{0:T(512)S(1)} %add_rsqrt_fusion.2), kind=kOutput, calls=%fused_computation.17 | convolution fusion | flops 2418868224 | bytes 10233344 | tf_op jit(solution)/shard_map/dot_general | solution.py:25
  155.6 107.7 %all-gather.14.cloned.1.call-done = bf16[2048,1536]{1,0:T(8,128)(2,1)} async-done(((bf16[512,1536]{1,0:T(8,128)(2,1)}), bf16[2048,1536]{1,0:T(8,128)(2,1)}) %all-gather.14.cloned.1.call-update) | async-done | bytes 6291472 | tf_op jit(solution)/shard_map/all_gather | solution.py:52
  263.3 115.0 %all-gather.16.cloned.1.call-done = bf16[1536,2048]{1,0:T(8,128)(2,1)} async-done(((bf16[1536,512]{1,0:T(8,128)(2,1)}), bf16[1536,2048]{1,0:T(8,128)(2,1)}) %all-gather.16.cloned.1.call-update) | async-done | bytes 6291472 | tf_op jit(solution)/shard_map/all_gather | solution.py:58
  378.3 11.6 %convolution_convert_fusion.2 = bf16[384,2048]{1,0:T(8,128)(2,1)} fusion(bf16[1536,2048]{1,0:T(8,128)(2,1)} %all-gather.16.cloned.1.call-done, bf16[2048,1536]{1,0:T(8,128)(2,1)} %all-gather.14.cloned.1.call-done, f32[384,1536]{1,0:T(8,128)} %convolution_multiply_fusion.3, bf16[384,2048]{1,0:T(8,128)(2,1)S(1)} %copy-done.2, f32[2048]{0:T(1024)S(1)} %bitcast.39, ...), kind=kOutput, calls=%fused_computation.22 | convolution fusion | flops 4839112704 | bytes 18097664 | tf_op jit(solution)/shard_map/dot_general | solution.py:56
  389.9 0.0 all-gather.18.cloned.1.call-start
  390.0 26.3 %reduce-scatter.4.cloned.1.call-done = bf16[384,512]{1,0:T(8,128)(2,1)} async-done(((bf16[384,2048]{1,0:T(8,128)(2,1)}), bf16[384,512]{1,0:T(8,128)(2,1)}) %reduce-scatter.4.cloned.1.call-update) | async-done | bytes 393232 | tf_op jit(solution)/shard_map/reduce_scatter | solution.py:19
  416.3 1.9 add_convert_fusion.1
  418.2 0.0 all-gather.22.cloned.1.call-start
  418.2 0.7 all-gather.22.cloned.1.call-update
  419.0 0.7 all-gather.24.cloned.1.call-update
  419.7 0.7 all-gather.20.cloned.1.call-update
  420.4 0.0 reduce-scatter.6.cloned.1.call-start
  420.5 5.2 all_gather.45
  425.7 12.2 %all-gather.18.cloned.1.call-done = bf16[384,2048]{1,0:T(8,128)(2,1)} async-done(((bf16[384,512]{1,0:T(8,128)(2,1)}), bf16[384,2048]{1,0:T(8,128)(2,1)}) %all-gather.18.cloned.1.call-update) | async-done | bytes 1572880 | tf_op jit(solution)/shard_map/all_gather | solution.py:9
  437.9 1.8 fusion.2
  439.7 27.8 %all-gather.22.cloned.1.call-done = bf16[2048,256]{1,0:T(8,128)(2,1)} async-done(((bf16[512,256]{1,0:T(8,128)(2,1)}), bf16[2048,256]{1,0:T(8,128)(2,1)}) %all-gather.22.cloned.1.call-update) | async-done | bytes 1048592 | tf_op jit(solution)/shard_map/all_gather | solution.py:69
  467.5 2.5 fusion.45
  470.0 0.1 copy.15
  470.1 0.3 fusion.52
  470.5 0.1 broadcast_add_fusion
  470.6 0.1 copy.17
  470.7 0.6 fusion.69
  471.3 0.1 copy-done.10
  471.3 0.1 fusion.67
  471.5 25.0 %all-gather.24.cloned.1.call-done = bf16[256,2048]{1,0:T(8,128)(2,1)} async-done(((bf16[256,512]{1,0:T(8,128)(2,1)}), bf16[256,2048]{1,0:T(8,128)(2,1)}) %all-gather.24.cloned.1.call-update) | async-done | bytes 1048592 | tf_op jit(solution)/shard_map/all_gather | solution.py:94
  496.5 3.0 convolution_convert_fusion.1
  499.5 0.0 all-gather.26.cloned.1.call-start
  499.5 43.6 %all-gather.20.cloned.1.call-done = bf16[2048,512]{1,0:T(8,128)(2,1)} async-done(((bf16[512,512]{1,0:T(8,128)(2,1)}), bf16[2048,512]{1,0:T(8,128)(2,1)}) %all-gather.20.cloned.1.call-update) | async-done | bytes 2097168 | tf_op jit(solution)/shard_map/all_gather | solution.py:70
  543.1 29.2 %reduce-scatter.6.cloned.1.call-done = bf16[384,512]{1,0:T(8,128)(2,1)} async-done(((bf16[384,2048]{1,0:T(8,128)(2,1)}), bf16[384,512]{1,0:T(8,128)(2,1)}) %reduce-scatter.6.cloned.1.call-update) | async-done | bytes 393232 | tf_op jit(solution)/shard_map/reduce_scatter | solution.py:19
  572.4 3.5 fusion.42
  575.9 0.0 reduce-scatter.8.cloned.1.call-start
  576.0 5.4 all_gather.50
  581.4 14.3 %all-gather.26.cloned.1.call-done = bf16[384,2048]{1,0:T(8,128)(2,1)} async-done(((bf16[384,512]{1,0:T(8,128)(2,1)}), bf16[384,2048]{1,0:T(8,128)(2,1)}) %all-gather.26.cloned.1.call-update) | async-done | bytes 1572880 | tf_op jit(solution)/shard_map/all_gather | solution.py:9
  595.7 1.8 fusion.4
  597.5 7.4 %convolution_multiply_fusion.1 = f32[384,1536]{1,0:T(8,128)} fusion(bf16[2048,1536]{1,0:T(8,128)(2,1)} %all-gather.12.cloned.1.call-done, bf16[384,2048]{1,0:T(8,128)(2,1)} %all-gather.26.cloned.1.call-done, f32[2048]{0:T(1024)S(1)} %bitcast.40, f32[384]{0:T(512)S(1)} %add_rsqrt_fusion), kind=kOutput, calls=%fused_computation.14 | convolution fusion | flops 2418868224 | bytes 10233344 | tf_op jit(solution)/shard_map/dot_general | solution.py:25
  604.9 11.6 %convolution_convert_fusion = bf16[384,2048]{1,0:T(8,128)(2,1)} fusion(bf16[1536,2048]{1,0:T(8,128)(2,1)} %all-gather.16.cloned.1.call-done, bf16[2048,1536]{1,0:T(8,128)(2,1)} %all-gather.14.cloned.1.call-done, f32[384,1536]{1,0:T(8,128)} %convolution_multiply_fusion.1, bf16[384,2048]{1,0:T(8,128)(2,1)S(1)} %copy-done.3, f32[2048]{0:T(1024)S(1)} %bitcast.41, ...), kind=kOutput, calls=%fused_computation.20 | convolution fusion | flops 4839112704 | bytes 18097664 | tf_op jit(solution)/shard_map/dot_general | solution.py:56
  616.6 28.1 %reduce-scatter.8.cloned.1.call-done = bf16[384,512]{1,0:T(8,128)(2,1)} async-done(((bf16[384,2048]{1,0:T(8,128)(2,1)}), bf16[384,512]{1,0:T(8,128)(2,1)}) %reduce-scatter.8.cloned.1.call-update) | async-done | bytes 393232 | tf_op jit(solution)/shard_map/reduce_scatter | solution.py:19
  644.7 1.9 add_convert_fusion
  (43 shorter events, 0.4 us)
Async XLA Ops:
  6.5 464.1 %copy-start = (bf16[2,128,128]{2,1,0:T(8,128)(2,1)S(1)}, bf16[2,128,128]{2,1,0:T(8,128)(2,1)}, u32[]{:S(2)}) copy-start(bf16[2,128,128]{2,1,0:T(8,128)(2,1)} %param.20) | copy-start | bytes 196612
  6.5 24.7 %all-gather.10.cloned.1.call-start = ((), (), s32[]{:S(2)}) async-start(), calls=%async_computation.3 | async-start | bytes 1966080 | tf_op jit(solution)/shard_map/all_gather | solution.py:9
  7.3 2.1 copy-start.7
  7.3 140.9 %all-gather.12.cloned.1.call-start = ((), (), s32[]{:S(2)}) async-start(), calls=%async_computation.4 | async-start | bytes 7864320 | tf_op jit(solution)/shard_map/all_gather | solution.py:51
  8.0 255.3 %all-gather.14.cloned.1.call-start = ((), (), s32[]{:S(2)}) async-start(), calls=%async_computation.5 | async-start | bytes 7864320 | tf_op jit(solution)/shard_map/all_gather | solution.py:52
  8.8 369.6 %all-gather.16.cloned.1.call-start = ((), (), s32[]{:S(2)}) async-start(), calls=%async_computation.6 | async-start | bytes 7864320 | tf_op jit(solution)/shard_map/all_gather | solution.py:58
  9.3 406.9 %reduce-scatter.4.cloned.1.call-start = ((), (), s32[]{:S(2)}) async-start(), calls=%async_computation.7 | async-start | bytes 1966080 | tf_op jit(solution)/shard_map/reduce_scatter | solution.py:19
  148.2 230.1 %copy-start.2 = (bf16[384,2048]{1,0:T(8,128)(2,1)S(1)}, bf16[384,2048]{1,0:T(8,128)(2,1)}, u32[]{:S(2)}) copy-start(bf16[384,2048]{1,0:T(8,128)(2,1)} %all-gather.10.cloned.1.call-done) | copy-start | bytes 4718596
  155.6 260.7 %copy-start.4 = (bf16[384,512]{1,0:T(8,128)(2,1)S(1)}, bf16[384,512]{1,0:T(8,128)(2,1)}, u32[]{:S(2)}) copy-start(bf16[384,512]{1,0:T(8,128)(2,1)} %param.12) | copy-start | bytes 1179652
  389.9 30.5 %copy-start.8 = (bf16[1,512]{1,0:T(2,128)(2,1)S(1)}, bf16[1,512]{1,0:T(2,128)(2,1)}, u32[]{:S(2)}) copy-start(bf16[1,512]{1,0:T(2,128)(2,1)} %param.17) | copy-start | bytes 3076
  389.9 48.0 %all-gather.18.cloned.1.call-start = ((), (), s32[]{:S(2)}) async-start(), calls=%async_computation.8 | async-start | bytes 1966080 | tf_op jit(solution)/shard_map/all_gather | solution.py:9
  418.2 49.4 %all-gather.22.cloned.1.call-start = ((), (), s32[]{:S(2)}) async-start(), calls=%async_computation.10 | async-start | bytes 1310720 | tf_op jit(solution)/shard_map/all_gather | solution.py:69
  418.9 77.6 %all-gather.24.cloned.1.call-start = ((), (), s32[]{:S(2)}) async-start(), calls=%async_computation.11 | async-start | bytes 1310720 | tf_op jit(solution)/shard_map/all_gather | solution.py:94
  419.7 123.5 %all-gather.20.cloned.1.call-start = ((), (), s32[]{:S(2)}) async-start(), calls=%async_computation.9 | async-start | bytes 2621440 | tf_op jit(solution)/shard_map/all_gather | solution.py:70
  420.4 152.0 %reduce-scatter.6.cloned.1.call-start = ((), (), s32[]{:S(2)}) async-start(), calls=%async_computation.12 | async-start | bytes 1966080 | tf_op jit(solution)/shard_map/reduce_scatter | solution.py:19
  470.7 0.7 copy-start.10
  471.3 101.0 %copy-start.1 = (bf16[384,2048]{1,0:T(8,128)(2,1)S(1)}, bf16[384,2048]{1,0:T(8,128)(2,1)}, u32[]{:S(2)}) copy-start(bf16[384,2048]{1,0:T(8,128)(2,1)} %all-gather.18.cloned.1.call-done) | copy-start | bytes 4718596
  471.3 101.0 %copy-start.5 = (bf16[384,512]{1,0:T(8,128)(2,1)S(1)}, bf16[384,512]{1,0:T(8,128)(2,1)}, u32[]{:S(2)}) copy-start(bf16[384,512]{1,0:T(8,128)(2,1)} %add_convert_fusion.1) | copy-start | bytes 1179652
  499.5 76.5 %copy-start.9 = (bf16[1,512]{1,0:T(2,128)(2,1)S(1)}, bf16[1,512]{1,0:T(2,128)(2,1)}, u32[]{:S(2)}) copy-start(bf16[1,512]{1,0:T(2,128)(2,1)} %param.23) | copy-start | bytes 3076
  499.5 96.2 %all-gather.26.cloned.1.call-start = ((), (), s32[]{:S(2)}) async-start(), calls=%async_computation.13 | async-start | bytes 1966080 | tf_op jit(solution)/shard_map/all_gather | solution.py:9
  575.9 68.8 %reduce-scatter.8.cloned.1.call-start = ((), (), s32[]{:S(2)}) async-start(), calls=%async_computation.14 | async-start | bytes 1966080 | tf_op jit(solution)/shard_map/reduce_scatter | solution.py:19
  597.5 7.4 %copy-start.3 = (bf16[384,2048]{1,0:T(8,128)(2,1)S(1)}, bf16[384,2048]{1,0:T(8,128)(2,1)}, u32[]{:S(2)}) copy-start(bf16[384,2048]{1,0:T(8,128)(2,1)} %all-gather.26.cloned.1.call-done) | copy-start | bytes 4718596
  604.9 39.8 %copy-start.6 = (bf16[384,512]{1,0:T(8,128)(2,1)S(1)}, bf16[384,512]{1,0:T(8,128)(2,1)}, u32[]{:S(2)}) copy-start(bf16[384,512]{1,0:T(8,128)(2,1)} %fusion.42) | copy-start | bytes 1179652
Sparse Core Ops, SparseCore 0:
  8.9 22.3 all-gather.9
  32.9 115.3 all-gather.11
  149.8 113.5 all-gather.13
  264.8 113.4 all-gather.15
  390.1 26.1 reduce-scatter.3
  418.3 19.6 all-gather.17
  439.5 27.9 all-gather.21
  469.1 27.3 all-gather.23
  498.1 45.0 all-gather.19
  545.5 26.8 reduce-scatter.5
  576.0 19.6 all-gather.25
  616.7 27.9 reduce-scatter.7
where the time goes:
time: 654 us; the launch traced here: 653 us
  waiting for transfers between devices  565 us (86%)
  matrix products  47.6 us (7%)
  blocking collectives  16.7 us (3%)
  between operations  13.7 us (2%)
  other arithmetic  9.71 us (1%)
    all_gather x1, waiting for transfers between devices, feed_forward(): lax.all_gather(ffn_gate_w, 'fs', axis=0, tiled=True)  115 us
    all_gather x1, waiting for transfers between devices, feed_forward(): lax.all_gather(ffn_down_w, 'fs', axis=1, tiled=True)  115 us
    all_gather x1, waiting for transfers between devices, feed_forward(): lax.all_gather(ffn_up_w, 'fs', axis=0, tiled=True)  108 us
    reduce_scatter x3, waiting for transfers between devices, column_sums(): lax.psum_scatter(partial_value.astype(jnp.bfloat16), 'tp', scatter_dimens...  83.7 us
    all_gather x1, waiting for transfers between devices, per_device(): lax.all_gather(mixer_gate_w, 'fs', axis=0, tiled=True)  43.6 us
    all_gather x3, waiting for transfers between devices, norm_rows(): lax.all_gather(values, 'tp', axis=1, tiled=True)  42.2 us
    all_gather x1, waiting for transfers between devices, per_device(): lax.all_gather(pool_in_w, 'fs', axis=0, tiled=True)  27.8 us
    all_gather x1, waiting for transfers between devices, per_device(): lax.all_gather(mixer_out_w, 'fs', axis=1, tiled=True)  25 us
  transfers between devices with their start and end apart: 12, of which 12 were waited for; matrix products, arithmetic and copies ran while one was open for 3% of the time, Pallas kernels for 0%

commit v1 on v0

v1 whole, which is shorter than its diff:
```python
import jax
import jax.numpy as jnp
from jax import lax
from jax.sharding import PartitionSpec as P


def shift(size, step):
    return [(i, (i + step) % size) for i in range(size)]


def swap(size):
    return [(i, i ^ 1) for i in range(size)]


def per_device(
    layer_input,
    first_gain,
    ffn_gate_w,
    ffn_up_w,
    ffn_down_w,
    mixer_gain,
    pool_in_w,
    mixer_gate_w,
    group_mix_w,
    pool_scale,
    mixer_out_w,
    second_gain,
):
    n_grp, n_fs, n_tp = (lax.axis_size(name) for name in ("grp", "fs", "tp"))
    n_chip = n_tp // 2
    y, z, t = (lax.axis_index(name) for name in ("grp", "fs", "tp"))
    chip, core = t // 2, t % 2
    rows, shard = layer_input.shape
    width = shard * n_tp
    block = width // n_fs

    def pieces_of(weight, axis):
        part = weight.shape[axis] // n_grp
        own = [
            lax.dynamic_slice_in_dim(weight, ((y - k) % n_grp) * part, part, axis)
            for k in range(n_grp)
        ]
        gathered, current = [own], own[0]
        for _ in range(n_fs - 1):
            current = lax.ppermute(current, "fs", shift(n_fs, 1))
            gathered.append(
                [current] + [lax.ppermute(current, "grp", shift(n_grp, k)) for k in range(1, n_grp)]
            )
        return gathered

    def absolute(weight, axis, split):
        gathered = pieces_of(weight, split)
        shape = list(weight.shape)
        shape[axis] *= n_fs
        whole = jnp.zeros(shape, weight.dtype)
        for s, parts in enumerate(gathered):
            for k, part in enumerate(parts):
                start = [0, 0]
                start[axis] = ((z - s) % n_fs) * weight.shape[axis]
                start[split] = start[split] + ((y - k) % n_grp) * part.shape[split]
                whole = lax.dynamic_update_slice(whole, part, start)
        return whole

    def gather_tp(value):
        pieces = [(t, value), (t ^ 1, lax.ppermute(value, "tp", swap(n_tp)))]
        for k in range(1, n_chip):
            far = lax.ppermute(value, "tp", shift(n_tp, 2 * k))
            source = (t - 2 * k) % n_tp
            pieces.append((source, far))
            pieces.append((source ^ 1, lax.ppermute(far, "tp", swap(n_tp))))
        whole = jnp.zeros((value.shape[0], value.shape[1] * n_tp), value.dtype)
        for source, piece in pieces:
            whole = lax.dynamic_update_slice(whole, piece, (0, source * value.shape[1]))
        return whole

    def scatter_tp(partial):
        def at(index):
            return lax.dynamic_slice_in_dim(partial, index * shard, shard, 1)

        total = None
        for k in list(range(1, n_chip)) + [0]:
            there = ((chip + k) % n_chip) * 2
            other = lax.ppermute(at(there + (1 - core)), "tp", swap(n_tp))
            pair = at(there + core).astype(jnp.float32) + other.astype(jnp.float32)
            if k:
                pair = lax.ppermute(
                    pair.astype(jnp.bfloat16), "tp", shift(n_tp, 2 * k)
                ).astype(jnp.float32)
            total = pair if total is None else total + pair
        return total

    def norm_rows(values, gain):
        whole = gather_tp(values)
        gain_whole = lax.all_gather(gain, "tp", axis=1, tiled=True)
        widened = whole.astype(jnp.float32)
        scaled = (widened * gain_whole.astype(jnp.float32)).astype(jnp.bfloat16)
        factor = lax.rsqrt(jnp.mean(widened * widened, axis=1, keepdims=True) + 1e-06)
        return scaled, factor

    gate_pieces = pieces_of(ffn_gate_w, 1)
    up_pieces = pieces_of(ffn_up_w, 1)
    down_pieces = pieces_of(ffn_down_w, 0)

    def feed_forward(values, gain):
        scaled, factor = norm_rows(values, gain)
        inputs = [
            lax.dynamic_slice_in_dim(scaled, ((z - s) % n_fs) * block, block, 1)
            for s in range(n_fs)
        ]

        def project(gathered, k):
            total = None
            for s in range(n_fs):
                product = jnp.dot(inputs[s], gathered[s][k], preferred_element_type=jnp.float32)
                total = product if total is None else total + product
            return total

        hidden = [
            (
                jax.nn.silu(factor * project(gate_pieces, k)) * (factor * project(up_pieces, k))
            ).astype(jnp.bfloat16)
            for k in range(n_grp)
        ]
        out = jnp.zeros((rows, width), jnp.bfloat16)
        for s in range(n_fs):
            product = None
            for k in range(n_grp):
                term = jnp.dot(hidden[k], down_pieces[s][k], preferred_element_type=jnp.float32)
                product = term if product is None else product + term
            out = lax.dynamic_update_slice(
                out, product.astype(jnp.bfloat16), (0, ((z - s) % n_fs) * block)
            )
        return scatter_tp(out)

    first = (
        layer_input.astype(jnp.float32) + 0.5 * feed_forward(layer_input, first_gain)
    ).astype(jnp.bfloat16)

    pool_in = absolute(pool_in_w, 0, 0)
    mixer_gate = absolute(mixer_gate_w, 0, 0)
    mixer_out = absolute(mixer_out_w, 1, 0)
    scaled, factor = norm_rows(first, mixer_gain)
    pool_pre = (
        factor * jnp.dot(scaled, pool_in, preferred_element_type=jnp.float32)
    ).astype(jnp.bfloat16)
    gate_logit = factor * jnp.dot(scaled, mixer_gate, preferred_element_type=jnp.float32)
    groups, group_width = group_mix_w.shape[:2]
    position = lax.broadcasted_iota(jnp.int32, (rows, rows), 0)
    back = position - lax.broadcasted_iota(jnp.int32, (rows, rows), 1)
    row = lax.broadcasted_iota(jnp.int32, (rows, 1), 0)
    pooled = []
    for g in range(groups):
        window = 2 ** (1 + (t * groups + g) % 4)
        band = ((back >= 0) & (back < window)).astype(jnp.bfloat16)
        values = pool_pre[:, g * group_width : (g + 1) * group_width]
        sums = jnp.dot(band, values, preferred_element_type=jnp.float32)
        count = jnp.minimum(row + 1, window).astype(jnp.float32)
        trail = (sums / count - values.astype(jnp.float32)).astype(jnp.bfloat16)
        mixed = jnp.dot(trail, group_mix_w[g], preferred_element_type=jnp.float32)
        pooled.append(mixed)
    pooled = (jnp.concatenate(pooled, axis=1) * pool_scale).astype(jnp.bfloat16)
    lifted = scatter_tp(
        jnp.dot(pooled, mixer_out, preferred_element_type=jnp.float32).astype(jnp.bfloat16)
    )
    second = (first.astype(jnp.float32) + jax.nn.sigmoid(gate_logit) * lifted).astype(jnp.bfloat16)
    result = second.astype(jnp.float32) + 0.5 * feed_forward(second, second_gain)
    return result.astype(jnp.bfloat16)


def solution(mesh):
    return jax.shard_map(
        per_device,
        mesh=mesh,
        in_specs=(
            P(("grp", "fs"), "tp"),
            P(None, "tp"),
            P("fs", "tp"),
            P("fs", "tp"),
            P("tp", "fs"),
            P(None, "tp"),
            P("fs", "tp"),
            P("fs", "tp"),
            P("tp", None, None),
            P(None, "tp"),
            P("tp", "fs"),
            P(None, "tp"),
        ),
        out_specs=P(("grp", "fs"), "tp"),
        check_vma=False,
    )
```

time: 654 us -> 358 us (0.55)
  waiting for transfers between devices: 565 us -> 181 us
  local copies, waits for them, and re-layouts: 0.32 us -> 57.1 us
  starting transfers between devices: 0.44 us -> 46.8 us
  between operations: 13.7 us -> 1.2 us
    all_gather x9 -> x0, waiting for transfers between devices: 477 us -> none  [the longest x1 115 us: feed_forward(): lax.all_gather(ffn_gate_w, 'fs', axis=0, tiled=True)]
    ppermute x0 -> x54, waiting for transfers between devices: none -> 181 us  [the longest x18 114 us: pieces_of(): current = lax.ppermute(current, 'fs', shift(n_fs, 1))]
    reduce_scatter x3 -> x0, waiting for transfers between devices: 83.7 us -> none  [column_sums(): lax.psum_scatter(partial_value.astype(jnp.bfloat16), 'tp', scatter_dimens...]
    ppermute x0 -> x54, starting transfers between devices: none -> 46.8 us  [the longest x18 22.2 us: pieces_of(): lax.ppermute(current, 'grp', shift(n_grp, k))]
    dynamic_update_slice x0 -> x33, local copies, waits for them, and re-layouts: none -> 36.7 us  [the longest x23 33.3 us: absolute(): whole = lax.dynamic_update_slice(whole, part, start)]
    unnamed x22 -> x100, local copies, waits for them, and re-layouts: 0.1 us -> 10.8 us
    dot_general x8 -> x53, matrix products: 47.6 us -> 42.7 us  [the longest x32 20.7 us: project(): jnp.dot(inputs[s], gathered[s][k], preferred_element_type=jnp.float32)]
  transfers between devices with their start and end apart: 12 -> 54, of which waited for: 12 -> 20; matrix products, arithmetic and copies ran while one was open for 3% -> 20% of each run, Pallas kernels for 0% -> 0%
where the time goes in v1:
time: 358 us; the launch traced here: 357 us
  waiting for transfers between devices  181 us (51%)
  local copies, waits for them, and re-layouts  57.1 us (16%)
  starting transfers between devices  46.8 us (13%)
  matrix products  42.7 us (12%)
  blocking collectives  21.1 us (6%)
  other arithmetic  6.21 us (2%)
    ppermute x18, waiting for transfers between devices, pieces_of(): current = lax.ppermute(current, 'fs', shift(n_fs, 1))  114 us
    ppermute x18, waiting for transfers between devices, pieces_of(): lax.ppermute(current, 'grp', shift(n_grp, k))  38.5 us
    dynamic_update_slice x23, local copies, waits for them, and re-layouts, absolute(): whole = lax.dynamic_update_slice(whole, part, start)  33.3 us
    ppermute x18, starting transfers between devices, pieces_of(): lax.ppermute(current, 'grp', shift(n_grp, k))  22.2 us
    all_gather x3, blocking collectives, norm_rows(): gain_whole = lax.all_gather(gain, 'tp', axis=1, tiled=True)  21.1 us
    dot_general x32, matrix products, project(): jnp.dot(inputs[s], gathered[s][k], preferred_element_type=jnp.float32)  20.7 us
    ppermute x18, starting transfers between devices, pieces_of(): current = lax.ppermute(current, 'fs', shift(n_fs, 1))  15.6 us
    ppermute x3, waiting for transfers between devices, gather_tp(): far = lax.ppermute(value, 'tp', shift(n_tp, 2 * k))  14.2 us
  transfers between devices with their start and end apart: 54, of which 20 were waited for; matrix products, arithmetic and copies ran while one was open for 20% of the time, Pallas kernels for 0%

profile of v1, /device:TPU:0, one launch (start us, length us, event | category | flops | bytes accessed | tf_op | source)
XLA Modules:
  0.0 356.5 jit_solution(13257093705416114040)
XLA Ops:
  0.0 3.0 collective-permute-start.1
  4.3 1.6 collective-permute-start.3
  6.0 1.6 collective-permute-start.6
  7.6 4.8 %collective-permute-done.1 = bf16[384,512]{1,0:T(8,128)(2,1)} collective-permute-done((bf16[384,512]{1,0:T(8,128)(2,1)}, bf16[384,512]{1,0:T(8,128)(2,1)}, u32[]{:S(2)}, u32[]{:S(2)}) %collective-permute-start.1) | collective-permute-done | bytes 393248 | tf_op jit(solution)/shard_map/ppermute | solution.py:67
  13.4 1.8 collective-permute-start.15
  15.2 5.2 %all_gather.9 = bf16[1,2048]{1,0:T(2,128)(2,1)S(1)} all-gather(bf16[1,512]{1,0:T(2,128)(2,1)S(1)} %copy-done.40), channel_id=1, replica_groups=mesh['grp'=2,'fs'=4,'tp'=4] {'tp'}, dimensions={1}, use_global_device_ids=true | all-gather | bytes 5120 | tf_op jit(solution)/shard_map/all_gather | solution.py:94
  22.9 3.8 %collective-permute-done.3 = bf16[512,768]{1,0:T(8,128)(2,1)} collective-permute-done((bf16[512,768]{1,0:T(8,128)(2,1)S(1)}, bf16[512,768]{1,0:T(8,128)(2,1)}, u32[]{:S(2)}, u32[]{:S(2)}) %collective-permute-start.3) | collective-permute-done | bytes 786464 | tf_op jit(solution)/shard_map/ppermute | solution.py:45
  30.8 12.8 %collective-permute-done.6 = bf16[512,768]{1,0:T(8,128)(2,1)} collective-permute-done((bf16[512,768]{1,0:T(8,128)(2,1)S(1)}, bf16[512,768]{1,0:T(8,128)(2,1)}, u32[]{:S(2)}, u32[]{:S(2)}) %collective-permute-start.6) | collective-permute-done | bytes 786464 | tf_op jit(solution)/shard_map/ppermute | solution.py:45
  45.6 1.7 fusion.126
  49.4 10.9 %collective-permute-done.15 = bf16[768,512]{1,0:T(8,128)(2,1)} collective-permute-done((bf16[768,512]{1,0:T(8,128)(2,1)}, bf16[768,512]{1,0:T(8,128)(2,1)}, u32[]{:S(2)}, u32[]{:S(2)}) %collective-permute-start.15) | collective-permute-done | bytes 786464 | tf_op jit(solution)/shard_map/ppermute | solution.py:45
  62.0 15.1 %collective-permute-done.4 = bf16[512,768]{1,0:T(8,128)(2,1)S(1)} collective-permute-done((bf16[512,768]{1,0:T(8,128)(2,1)}, bf16[512,768]{1,0:T(8,128)(2,1)S(1)}, u32[]{:S(2)}, u32[]{:S(2)}) %collective-permute-start.4) | collective-permute-done | bytes 786464 | tf_op jit(solution)/shard_map/ppermute | solution.py:45
  79.6 14.4 %collective-permute-done.7 = bf16[512,768]{1,0:T(8,128)(2,1)S(1)} collective-permute-done((bf16[512,768]{1,0:T(8,128)(2,1)}, bf16[512,768]{1,0:T(8,128)(2,1)S(1)}, u32[]{:S(2)}, u32[]{:S(2)}) %collective-permute-start.7) | collective-permute-done | bytes 786464 | tf_op jit(solution)/shard_map/ppermute | solution.py:45
  96.3 14.5 %collective-permute-done.17 = bf16[768,512]{1,0:T(8,128)(2,1)S(1)} collective-permute-done((bf16[768,512]{1,0:T(8,128)(2,1)}, bf16[768,512]{1,0:T(8,128)(2,1)S(1)}, u32[]{:S(2)}, u32[]{:S(2)}) %collective-permute-start.17) | collective-permute-done | bytes 786464 | tf_op jit(solution)/shard_map/ppermute | solution.py:45
  113.5 14.2 %collective-permute-done.5 = bf16[512,768]{1,0:T(8,128)(2,1)S(1)} collective-permute-done((bf16[512,768]{1,0:T(8,128)(2,1)S(1)}, bf16[512,768]{1,0:T(8,128)(2,1)S(1)}, u32[]{:S(2)}, u32[]{:S(2)}) %collective-permute-start.5) | collective-permute-done | bytes 786464 | tf_op jit(solution)/shard_map/ppermute | solution.py:45
  128.2 16.3 %collective-permute-done.8 = bf16[512,768]{1,0:T(8,128)(2,1)S(1)} collective-permute-done((bf16[512,768]{1,0:T(8,128)(2,1)S(1)}, bf16[512,768]{1,0:T(8,128)(2,1)S(1)}, u32[]{:S(2)}, u32[]{:S(2)}) %collective-permute-start.8) | collective-permute-done | bytes 786464 | tf_op jit(solution)/shard_map/ppermute | solution.py:45
  150.4 9.6 %collective-permute-done.19 = bf16[768,512]{1,0:T(8,128)(2,1)S(1)} collective-permute-done((bf16[768,512]{1,0:T(8,128)(2,1)S(1)}, bf16[768,512]{1,0:T(8,128)(2,1)S(1)}, u32[]{:S(2)}, u32[]{:S(2)}) %collective-permute-start.19) | collective-permute-done | bytes 786464 | tf_op jit(solution)/shard_map/ppermute | solution.py:45
  164.0 16.4 %collective-permute-done.14 = bf16[512,768]{1,0:T(8,128)(2,1)S(1)} collective-permute-done((bf16[512,768]{1,0:T(8,128)(2,1)S(1)}, bf16[512,768]{1,0:T(8,128)(2,1)S(1)}, u32[]{:S(2)}, u32[]{:S(2)}) %collective-permute-start.14) | collective-permute-done | bytes 786464 | tf_op jit(solution)/shard_map/ppermute | solution.py:47
  183.0 12.1 %collective-permute-done.20 = bf16[768,512]{1,0:T(8,128)(2,1)S(1)} collective-permute-done((bf16[768,512]{1,0:T(8,128)(2,1)S(1)}, bf16[768,512]{1,0:T(8,128)(2,1)S(1)}, u32[]{:S(2)}, u32[]{:S(2)}) %collective-permute-start.20) | collective-permute-done | bytes 786464 | tf_op jit(solution)/shard_map/ppermute | solution.py:47
  201.5 1.6 constant_dynamic-slice_fusion.3
  208.2 2.0 add_convert_fusion.4
  212.4 10.5 %all_gather.10 = bf16[1,2048]{1,0:T(2,128)(2,1)S(1)} all-gather(bf16[1,512]{1,0:T(2,128)(2,1)S(1)} %copy-done.41), channel_id=1, replica_groups=mesh['grp'=2,'fs'=4,'tp'=4] {'tp'}, dimensions={1}, use_global_device_ids=true | all-gather | bytes 5120 | tf_op jit(solution)/shard_map/all_gather | solution.py:94
  226.1 2.1 collective-permute-start.35
  233.0 2.9 dynamic_update_slice.162
  237.3 2.3 collective-permute-start.37
  241.0 2.0 dynamic_update_slice.163
  243.0 3.4 dynamic_update_slice.164
  250.9 1.9 collective-permute-done.42
  252.8 1.7 collective-permute-start.29
  254.5 2.1 dynamic_update_slice.165
  256.6 3.4 dynamic_update_slice.166
  259.9 2.1 dynamic_update_slice.167
  264.0 2.5 fusion.61
  269.2 1.9 convolution_convert_fusion
  271.3 3.4 collective-permute-start.28
  275.4 1.7 constant_dynamic-update-slice_fusion.16
  277.1 4.9 %collective-permute-done.28 = bf16[256,512]{1,0:T(8,128)(2,1)S(1)} collective-permute-done((bf16[256,512]{1,0:T(8,128)(2,1)}, bf16[256,512]{1,0:T(8,128)(2,1)S(1)}, u32[]{:S(2)}, u32[]{:S(2)}) %collective-permute-start.28) | collective-permute-done | bytes 262176 | tf_op jit(solution)/shard_map/ppermute | solution.py:47
  282.7 2.3 collective-permute-done.31
  286.7 1.7 constant_dynamic-update-slice_fusion.14
  289.9 3.1 collective-permute-done.32
  293.7 3.3 collective-permute-done.46
  297.3 2.8 constant_dynamic-update-slice_fusion.3
  301.4 9.4 %collective-permute-done.49 = bf16[384,512]{1,0:T(8,128)(2,1)S(1)} collective-permute-done((bf16[384,512]{1,0:T(8,128)(2,1)S(1)}, bf16[384,512]{1,0:T(8,128)(2,1)S(1)}, u32[]{:S(2)}, u32[]{:S(2)}) %collective-permute-start.49) | collective-permute-done | bytes 393248 | tf_op jit(solution)/shard_map/ppermute | solution.py:67
  310.8 5.4 %all_gather.11 = bf16[1,2048]{1,0:T(2,128)(2,1)S(1)} all-gather(bf16[1,512]{1,0:T(2,128)(2,1)S(1)} %copy-done.42), channel_id=1, replica_groups=mesh['grp'=2,'fs'=4,'tp'=4] {'tp'}, dimensions={1}, use_global_device_ids=true | all-gather | bytes 5120 | tf_op jit(solution)/shard_map/all_gather | solution.py:94
  320.0 1.7 fusion.104
  323.3 1.7 fusion.102
  326.8 1.7 fusion.202
  335.4 1.7 fusion.203
  345.4 10.1 %collective-permute-done.52 = bf16[384,512]{1,0:T(8,128)(2,1)S(1)} collective-permute-done((bf16[384,512]{1,0:T(8,128)(2,1)S(1)}, bf16[384,512]{1,0:T(8,128)(2,1)S(1)}, u32[]{:S(2)}, u32[]{:S(2)}) %collective-permute-start.52) | collective-permute-done | bytes 393248 | tf_op jit(solution)/shard_map/ppermute | solution.py:86
  (280 shorter events, 98.2 us)
Async XLA Ops:
  0.0 12.4 %collective-permute-start.1 = (bf16[384,512]{1,0:T(8,128)(2,1)}, bf16[384,512]{1,0:T(8,128)(2,1)}, u32[]{:S(2)}, u32[]{:S(2)}) collective-permute-start(bf16[384,512]{1,0:T(8,128)(2,1)} %param.12), channel_id=1, source_target_pairs={{0,2},{1,3},{2,0},{3,1},{4,6},{5,7},{6,4},{7,5},{8,10},{9,11},{10,... | collective-permute-start | bytes 1179656 | tf_op jit(solution)/shard_map/ppermute | solution.py:67
  4.3 22.4 %collective-permute-start.3 = (bf16[512,768]{1,0:T(8,128)(2,1)S(1)}, bf16[512,768]{1,0:T(8,128)(2,1)}, u32[]{:S(2)}, u32[]{:S(2)}) collective-permute-start(bf16[512,768]{1,0:T(8,128)(2,1)S(1)} %constant_dynamic-slice_fusion.11), channel_id=1, source_target_pairs={{0,4},{4,8},{8,12},{12,0},{1,5},{5,9},{9,13},{13,1},{2,6},{6,10},{... | collective-permute-start | bytes 2359304 | tf_op jit(solution)/shard_map/ppermute | solution.py:45
  5.9 14.8 %collective-permute-start = (bf16[384,512]{1,0:T(8,128)(2,1)}, bf16[384,512]{1,0:T(8,128)(2,1)}, u32[]{:S(2)}, u32[]{:S(2)}) collective-permute-start(bf16[384,512]{1,0:T(8,128)(2,1)} %param.12), channel_id=1, source_target_pairs={{0,1},{1,0},{2,3},{3,2},{4,5},{5,4},{6,7},{7,6},{8,9},{9,8},{10,11... | collective-permute-start | bytes 1179656 | tf_op jit(solution)/shard_map/ppermute | solution.py:65
  6.0 37.5 %collective-permute-start.6 = (bf16[512,768]{1,0:T(8,128)(2,1)S(1)}, bf16[512,768]{1,0:T(8,128)(2,1)}, u32[]{:S(2)}, u32[]{:S(2)}) collective-permute-start(bf16[512,768]{1,0:T(8,128)(2,1)S(1)} %constant_dynamic-slice_fusion.10), channel_id=1, source_target_pairs={{0,4},{4,8},{8,12},{12,0},{1,5},{5,9},{9,13},{13,1},{2,6},{6,10},{... | collective-permute-start | bytes 2359304 | tf_op jit(solution)/shard_map/ppermute | solution.py:45
  12.4 15.8 %collective-permute-start.2 = (bf16[384,512]{1,0:T(8,128)(2,1)}, bf16[384,512]{1,0:T(8,128)(2,1)}, u32[]{:S(2)}, u32[]{:S(2)}) collective-permute-start(bf16[384,512]{1,0:T(8,128)(2,1)} %collective-permute-done.1), channel_id=1, source_target_pairs={{0,1},{1,0},{2,3},{3,2},{4,5},{5,4},{6,7},{7,6},{8,9},{9,8},{10,11... | collective-permute-start | bytes 1179656 | tf_op jit(solution)/shard_map/ppermute | solution.py:70
  13.4 47.0 %collective-permute-start.15 = (bf16[768,512]{1,0:T(8,128)(2,1)}, bf16[768,512]{1,0:T(8,128)(2,1)}, u32[]{:S(2)}, u32[]{:S(2)}) collective-permute-start(bf16[768,512]{1,0:T(8,128)(2,1)} %constant_dynamic-slice_fusion.9), channel_id=1, source_target_pairs={{0,4},{4,8},{8,12},{12,0},{1,5},{5,9},{9,13},{13,1},{2,6},{6,10},{... | collective-permute-start | bytes 2359304 | tf_op jit(solution)/shard_map/ppermute | solution.py:45
  26.7 35.2 %collective-permute-start.9 = (bf16[512,768]{1,0:T(8,128)(2,1)}, bf16[512,768]{1,0:T(8,128)(2,1)S(1)}, u32[]{:S(2)}, u32[]{:S(2)}) collective-permute-start(bf16[512,768]{1,0:T(8,128)(2,1)} %collective-permute-done.3), channel_id=1, source_target_pairs={{0,16},{16,0},{1,17},{17,1},{2,18},{18,2},{3,19},{19,3},{4,20},{20... | collective-permute-start | bytes 2359304 | tf_op jit(solution)/shard_map/ppermute | solution.py:47
  28.2 48.9 %collective-permute-start.4 = (bf16[512,768]{1,0:T(8,128)(2,1)}, bf16[512,768]{1,0:T(8,128)(2,1)S(1)}, u32[]{:S(2)}, u32[]{:S(2)}) collective-permute-start(bf16[512,768]{1,0:T(8,128)(2,1)} %collective-permute-done.3), channel_id=1, source_target_pairs={{0,4},{4,8},{8,12},{12,0},{1,5},{5,9},{9,13},{13,1},{2,6},{6,10},{... | collective-permute-start | bytes 2359304 | tf_op jit(solution)/shard_map/ppermute | solution.py:45
  43.5 50.5 %collective-permute-start.7 = (bf16[512,768]{1,0:T(8,128)(2,1)}, bf16[512,768]{1,0:T(8,128)(2,1)S(1)}, u32[]{:S(2)}, u32[]{:S(2)}) collective-permute-start(bf16[512,768]{1,0:T(8,128)(2,1)} %collective-permute-done.6), channel_id=1, source_target_pairs={{0,4},{4,8},{8,12},{12,0},{1,5},{5,9},{9,13},{13,1},{2,6},{6,10},{... | collective-permute-start | bytes 2359304 | tf_op jit(solution)/shard_map/ppermute | solution.py:45
  47.9 46.6 %collective-permute-start.12 = (bf16[512,768]{1,0:T(8,128)(2,1)}, bf16[512,768]{1,0:T(8,128)(2,1)S(1)}, u32[]{:S(2)}, u32[]{:S(2)}) collective-permute-start(bf16[512,768]{1,0:T(8,128)(2,1)} %collective-permute-done.6), channel_id=1, source_target_pairs={{0,16},{16,0},{1,17},{17,1},{2,18},{18,2},{3,19},{19,3},{4,20},{20... | collective-permute-start | bytes 2359304 | tf_op jit(solution)/shard_map/ppermute | solution.py:47
  60.4 121.7 %collective-permute-start.16 = (bf16[768,512]{1,0:T(8,128)(2,1)}, bf16[768,512]{1,0:T(8,128)(2,1)S(1)}, u32[]{:S(2)}, u32[]{:S(2)}) collective-permute-start(bf16[768,512]{1,0:T(8,128)(2,1)} %collective-permute-done.15), channel_id=1, source_target_pairs={{0,16},{16,0},{1,17},{17,1},{2,18},{18,2},{3,19},{19,3},{4,20},{20... | collective-permute-start | bytes 2359304 | tf_op jit(solution)/shard_map/ppermute | solution.py:47
  61.9 48.9 %collective-permute-start.17 = (bf16[768,512]{1,0:T(8,128)(2,1)}, bf16[768,512]{1,0:T(8,128)(2,1)S(1)}, u32[]{:S(2)}, u32[]{:S(2)}) collective-permute-start(bf16[768,512]{1,0:T(8,128)(2,1)} %collective-permute-done.15), channel_id=1, source_target_pairs={{0,4},{4,8},{8,12},{12,0},{1,5},{5,9},{9,13},{13,1},{2,6},{6,10},{... | collective-permute-start | bytes 2359304 | tf_op jit(solution)/shard_map/ppermute | solution.py:45
  77.1 35.2 %collective-permute-start.10 = (bf16[512,768]{1,0:T(8,128)(2,1)S(1)}, bf16[512,768]{1,0:T(8,128)(2,1)S(1)}, u32[]{:S(2)}, u32[]{:S(2)}) collective-permute-start(bf16[512,768]{1,0:T(8,128)(2,1)S(1)} %collective-permute-done.4), channel_id=1, source_target_pairs={{0,16},{16,0},{1,17},{17,1},{2,18},{18,2},{3,19},{19,3},{4,20},{20... | collective-permute-start | bytes 2359304 | tf_op jit(solution)/shard_map/ppermute | solution.py:47
  94.0 33.7 %collective-permute-start.5 = (bf16[512,768]{1,0:T(8,128)(2,1)S(1)}, bf16[512,768]{1,0:T(8,128)(2,1)S(1)}, u32[]{:S(2)}, u32[]{:S(2)}) collective-permute-start(bf16[512,768]{1,0:T(8,128)(2,1)S(1)} %collective-permute-done.4), channel_id=1, source_target_pairs={{0,4},{4,8},{8,12},{12,0},{1,5},{5,9},{9,13},{13,1},{2,6},{6,10},{... | collective-permute-start | bytes 2359304 | tf_op jit(solution)/shard_map/ppermute | solution.py:45
  94.5 50.1 %collective-permute-start.8 = (bf16[512,768]{1,0:T(8,128)(2,1)S(1)}, bf16[512,768]{1,0:T(8,128)(2,1)S(1)}, u32[]{:S(2)}, u32[]{:S(2)}) collective-permute-start(bf16[512,768]{1,0:T(8,128)(2,1)S(1)} %collective-permute-done.7), channel_id=1, source_target_pairs={{0,4},{4,8},{8,12},{12,0},{1,5},{5,9},{9,13},{13,1},{2,6},{6,10},{... | collective-permute-start | bytes 2359304 | tf_op jit(solution)/shard_map/ppermute | solution.py:45
  110.8 51.2 %collective-permute-start.13 = (bf16[512,768]{1,0:T(8,128)(2,1)S(1)}, bf16[512,768]{1,0:T(8,128)(2,1)S(1)}, u32[]{:S(2)}, u32[]{:S(2)}) collective-permute-start(bf16[512,768]{1,0:T(8,128)(2,1)S(1)} %collective-permute-done.7), channel_id=1, source_target_pairs={{0,16},{16,0},{1,17},{17,1},{2,18},{18,2},{3,19},{19,3},{4,20},{20... | collective-permute-start | bytes 2359304 | tf_op jit(solution)/shard_map/ppermute | solution.py:47
  112.4 70.2 %collective-permute-start.18 = (bf16[768,512]{1,0:T(8,128)(2,1)S(1)}, bf16[768,512]{1,0:T(8,128)(2,1)S(1)}, u32[]{:S(2)}, u32[]{:S(2)}) collective-permute-start(bf16[768,512]{1,0:T(8,128)(2,1)S(1)} %collective-permute-done.17), channel_id=1, source_target_pairs={{0,16},{16,0},{1,17},{17,1},{2,18},{18,2},{3,19},{19,3},{4,20},{20... | collective-permute-start | bytes 2359304 | tf_op jit(solution)/shard_map/ppermute | solution.py:47
  127.7 32.4 %collective-permute-start.19 = (bf16[768,512]{1,0:T(8,128)(2,1)S(1)}, bf16[768,512]{1,0:T(8,128)(2,1)S(1)}, u32[]{:S(2)}, u32[]{:S(2)}) collective-permute-start(bf16[768,512]{1,0:T(8,128)(2,1)S(1)} %collective-permute-done.17), channel_id=1, source_target_pairs={{0,4},{4,8},{8,12},{12,0},{1,5},{5,9},{9,13},{13,1},{2,6},{6,10},{... | collective-permute-start | bytes 2359304 | tf_op jit(solution)/shard_map/ppermute | solution.py:45
  144.5 18.6 %collective-permute-start.11 = (bf16[512,768]{1,0:T(8,128)(2,1)S(1)}, bf16[512,768]{1,0:T(8,128)(2,1)S(1)}, u32[]{:S(2)}, u32[]{:S(2)}) collective-permute-start(bf16[512,768]{1,0:T(8,128)(2,1)S(1)} %collective-permute-done.5), channel_id=1, source_target_pairs={{0,16},{16,0},{1,17},{17,1},{2,18},{18,2},{3,19},{19,3},{4,20},{20... | collective-permute-start | bytes 2359304 | tf_op jit(solution)/shard_map/ppermute | solution.py:47
  160.0 20.4 %collective-permute-start.14 = (bf16[512,768]{1,0:T(8,128)(2,1)S(1)}, bf16[512,768]{1,0:T(8,128)(2,1)S(1)}, u32[]{:S(2)}, u32[]{:S(2)}) collective-permute-start(bf16[512,768]{1,0:T(8,128)(2,1)S(1)} %collective-permute-done.8), channel_id=1, source_target_pairs={{0,16},{16,0},{1,17},{17,1},{2,18},{18,2},{3,19},{19,3},{4,20},{20... | collective-permute-start | bytes 2359304 | tf_op jit(solution)/shard_map/ppermute | solution.py:47
  162.0 33.1 %collective-permute-start.20 = (bf16[768,512]{1,0:T(8,128)(2,1)S(1)}, bf16[768,512]{1,0:T(8,128)(2,1)S(1)}, u32[]{:S(2)}, u32[]{:S(2)}) collective-permute-start(bf16[768,512]{1,0:T(8,128)(2,1)S(1)} %collective-permute-done.19), channel_id=1, source_target_pairs={{0,16},{16,0},{1,17},{17,1},{2,18},{18,2},{3,19},{19,3},{4,20},{20... | collective-permute-start | bytes 2359304 | tf_op jit(solution)/shard_map/ppermute | solution.py:47
  197.7 10.6 %collective-permute-start.21 = (bf16[384,512]{1,0:T(8,128)(2,1)}, bf16[384,512]{1,0:T(8,128)(2,1)}, u32[]{:S(2)}, u32[]{:S(2)}) collective-permute-start(bf16[384,512]{1,0:T(8,128)(2,1)} %get-tuple-element.17), channel_id=1, source_target_pairs={{0,1},{1,0},{2,3},{3,2},{4,5},{5,4},{6,7},{7,6},{8,9},{9,8},{10,11... | collective-permute-start | bytes 1179656 | tf_op jit(solution)/shard_map/ppermute | solution.py:83
  200.4 24.2 %collective-permute-start.33 = (bf16[256,256]{1,0:T(8,128)(2,1)}, bf16[256,256]{1,0:T(8,128)(2,1)}, u32[]{:S(2)}, u32[]{:S(2)}) collective-permute-start(bf16[256,256]{1,0:T(8,128)(2,1)} %get-tuple-element.6), channel_id=1, source_target_pairs={{0,4},{4,8},{8,12},{12,0},{1,5},{5,9},{9,13},{13,1},{2,6},{6,10},{... | collective-permute-start | bytes 393224 | tf_op jit(solution)/shard_map/ppermute | solution.py:45
  203.1 23.0 %collective-permute-start.39 = (bf16[128,512]{1,0:T(8,128)(2,1)}, bf16[128,512]{1,0:T(8,128)(2,1)}, u32[]{:S(2)}, u32[]{:S(2)}) collective-permute-start(bf16[128,512]{1,0:T(8,128)(2,1)} %get-tuple-element.21), channel_id=1, source_target_pairs={{0,4},{4,8},{8,12},{12,0},{1,5},{5,9},{9,13},{13,1},{2,6},{6,10},{... | collective-permute-start | bytes 393224 | tf_op jit(solution)/shard_map/ppermute | solution.py:45
  206.6 33.7 %collective-permute-start.27 = (bf16[256,512]{1,0:T(8,128)(2,1)}, bf16[256,512]{1,0:T(8,128)(2,1)}, u32[]{:S(2)}, u32[]{:S(2)}) collective-permute-start(bf16[256,512]{1,0:T(8,128)(2,1)} %get-tuple-element.10), channel_id=1, source_target_pairs={{0,4},{4,8},{8,12},{12,0},{1,5},{5,9},{9,13},{13,1},{2,6},{6,10},{... | collective-permute-start | bytes 786440 | tf_op jit(solution)/shard_map/ppermute | solution.py:45
  208.2 20.0 %collective-permute-start.23 = (bf16[384,512]{1,0:T(8,128)(2,1)}, bf16[384,512]{1,0:T(8,128)(2,1)}, u32[]{:S(2)}, u32[]{:S(2)}) collective-permute-start(bf16[384,512]{1,0:T(8,128)(2,1)} %get-tuple-element.18), channel_id=1, source_target_pairs={{0,1},{1,0},{2,3},{3,2},{4,5},{5,4},{6,7},{7,6},{8,9},{9,8},{10,11... | collective-permute-start | bytes 1179656 | tf_op jit(solution)/shard_map/ppermute | solution.py:83
  210.2 18.6 %collective-permute-start.22 = (bf16[384,512]{1,0:T(8,128)(2,1)}, bf16[384,512]{1,0:T(8,128)(2,1)}, u32[]{:S(2)}, u32[]{:S(2)}) collective-permute-start(bf16[384,512]{1,0:T(8,128)(2,1)} %add_convert_fusion.4), channel_id=1, source_target_pairs={{0,2},{1,3},{2,0},{3,1},{4,6},{5,7},{6,4},{7,5},{8,10},{9,11},{10,... | collective-permute-start | bytes 1179656 | tf_op jit(solution)/shard_map/ppermute | solution.py:86
  226.1 9.7 %collective-permute-start.35 = (bf16[256,256]{1,0:T(8,128)(2,1)}, bf16[256,256]{1,0:T(8,128)(2,1)S(1)}, u32[]{:S(2)}, u32[]{:S(2)}) collective-permute-start(bf16[256,256]{1,0:T(8,128)(2,1)} %collective-permute-done.33), channel_id=1, source_target_pairs={{0,4},{4,8},{8,12},{12,0},{1,5},{5,9},{9,13},{13,1},{2,6},{6,10},{... | collective-permute-start | bytes 393224 | tf_op jit(solution)/shard_map/ppermute | solution.py:45
  228.2 9.1 %collective-permute-start.40 = (bf16[128,512]{1,0:T(8,128)(2,1)}, bf16[128,512]{1,0:T(8,128)(2,1)S(1)}, u32[]{:S(2)}, u32[]{:S(2)}) collective-permute-start(bf16[128,512]{1,0:T(8,128)(2,1)} %collective-permute-done.39), channel_id=1, source_target_pairs={{0,16},{16,0},{1,17},{17,1},{2,18},{18,2},{3,19},{19,3},{4,20},{20... | collective-permute-start | bytes 393224 | tf_op jit(solution)/shard_map/ppermute | solution.py:47
  228.7 10.9 %collective-permute-start.41 = (bf16[128,512]{1,0:T(8,128)(2,1)}, bf16[128,512]{1,0:T(8,128)(2,1)S(1)}, u32[]{:S(2)}, u32[]{:S(2)}) collective-permute-start(bf16[128,512]{1,0:T(8,128)(2,1)} %collective-permute-done.39), channel_id=1, source_target_pairs={{0,4},{4,8},{8,12},{12,0},{1,5},{5,9},{9,13},{13,1},{2,6},{6,10},{... | collective-permute-start | bytes 393224 | tf_op jit(solution)/shard_map/ppermute | solution.py:45
  230.5 19.7 %collective-permute-start.25 = (bf16[384,512]{1,0:T(8,128)(2,1)S(1)}, bf16[384,512]{1,0:T(8,128)(2,1)S(1)}, u32[]{:S(2)}, u32[]{:S(2)}) collective-permute-start(bf16[384,512]{1,0:T(8,128)(2,1)S(1)} %get-tuple-element.8), channel_id=1, source_target_pairs={{0,2},{1,3},{2,0},{3,1},{4,6},{5,7},{6,4},{7,5},{8,10},{9,11},{10,... | collective-permute-start | bytes 1179656 | tf_op jit(solution)/shard_map/ppermute | solution.py:67
  235.8 10.6 %collective-permute-start.36 = (bf16[256,256]{1,0:T(8,128)(2,1)S(1)}, bf16[256,256]{1,0:T(8,128)(2,1)S(1)}, u32[]{:S(2)}, u32[]{:S(2)}) collective-permute-start(bf16[256,256]{1,0:T(8,128)(2,1)S(1)} %collective-permute-done.35), channel_id=1, source_target_pairs={{0,16},{16,0},{1,17},{17,1},{2,18},{18,2},{3,19},{19,3},{4,20},{20... | collective-permute-start | bytes 393224 | tf_op jit(solution)/shard_map/ppermute | solution.py:47
  237.3 10.2 %collective-permute-start.37 = (bf16[256,256]{1,0:T(8,128)(2,1)S(1)}, bf16[256,256]{1,0:T(8,128)(2,1)S(1)}, u32[]{:S(2)}, u32[]{:S(2)}) collective-permute-start(bf16[256,256]{1,0:T(8,128)(2,1)S(1)} %collective-permute-done.35), channel_id=1, source_target_pairs={{0,4},{4,8},{8,12},{12,0},{1,5},{5,9},{9,13},{13,1},{2,6},{6,10},{... | collective-permute-start | bytes 393224 | tf_op jit(solution)/shard_map/ppermute | solution.py:45
  239.6 8.8 %collective-permute-start.43 = (bf16[128,512]{1,0:T(8,128)(2,1)S(1)}, bf16[128,512]{1,0:T(8,128)(2,1)S(1)}, u32[]{:S(2)}, u32[]{:S(2)}) collective-permute-start(bf16[128,512]{1,0:T(8,128)(2,1)S(1)} %collective-permute-done.41), channel_id=1, source_target_pairs={{0,4},{4,8},{8,12},{12,0},{1,5},{5,9},{9,13},{13,1},{2,6},{6,10},{... | collective-permute-start | bytes 393224 | tf_op jit(solution)/shard_map/ppermute | solution.py:45
  240.4 22.4 %collective-permute-start.24 = (bf16[384,512]{1,0:T(8,128)(2,1)S(1)}, bf16[384,512]{1,0:T(8,128)(2,1)S(1)}, u32[]{:S(2)}, u32[]{:S(2)}) collective-permute-start(bf16[384,512]{1,0:T(8,128)(2,1)S(1)} %get-tuple-element.8), channel_id=1, source_target_pairs={{0,1},{1,0},{2,3},{3,2},{4,5},{5,4},{6,7},{7,6},{8,9},{9,8},{10,11... | collective-permute-start | bytes 1179656 | tf_op jit(solution)/shard_map/ppermute | solution.py:65
  247.5 14.5 %collective-permute-start.38 = (bf16[256,256]{1,0:T(8,128)(2,1)S(1)}, bf16[256,256]{1,0:T(8,128)(2,1)S(1)}, u32[]{:S(2)}, u32[]{:S(2)}) collective-permute-start(bf16[256,256]{1,0:T(8,128)(2,1)S(1)} %collective-permute-done.37), channel_id=1, source_target_pairs={{0,16},{16,0},{1,17},{17,1},{2,18},{18,2},{3,19},{19,3},{4,20},{20... | collective-permute-start | bytes 393224 | tf_op jit(solution)/shard_map/ppermute | solution.py:47
  248.5 11.5 %collective-permute-start.44 = (bf16[128,512]{1,0:T(8,128)(2,1)S(1)}, bf16[128,512]{1,0:T(8,128)(2,1)S(1)}, u32[]{:S(2)}, u32[]{:S(2)}) collective-permute-start(bf16[128,512]{1,0:T(8,128)(2,1)S(1)} %collective-permute-done.43), channel_id=1, source_target_pairs={{0,16},{16,0},{1,17},{17,1},{2,18},{18,2},{3,19},{19,3},{4,20},{20... | collective-permute-start | bytes 393224 | tf_op jit(solution)/shard_map/ppermute | solution.py:47
  250.2 12.6 %collective-permute-start.26 = (bf16[384,512]{1,0:T(8,128)(2,1)S(1)}, bf16[384,512]{1,0:T(8,128)(2,1)S(1)}, u32[]{:S(2)}, u32[]{:S(2)}) collective-permute-start(bf16[384,512]{1,0:T(8,128)(2,1)S(1)} %collective-permute-done.25), channel_id=1, source_target_pairs={{0,1},{1,0},{2,3},{3,2},{4,5},{5,4},{6,7},{7,6},{8,9},{9,8},{10,11... | collective-permute-start | bytes 1179656 | tf_op jit(solution)/shard_map/ppermute | solution.py:70
  252.8 21.9 %collective-permute-start.29 = (bf16[256,512]{1,0:T(8,128)(2,1)}, bf16[256,512]{1,0:T(8,128)(2,1)}, u32[]{:S(2)}, u32[]{:S(2)}) collective-permute-start(bf16[256,512]{1,0:T(8,128)(2,1)} %collective-permute-done.27), channel_id=1, source_target_pairs={{0,4},{4,8},{8,12},{12,0},{1,5},{5,9},{9,13},{13,1},{2,6},{6,10},{... | collective-permute-start | bytes 786440 | tf_op jit(solution)/shard_map/ppermute | solution.py:45
  271.2 14.1 %collective-permute-start.45 = (bf16[384,512]{1,0:T(8,128)(2,1)S(1)}, bf16[384,512]{1,0:T(8,128)(2,1)S(1)}, u32[]{:S(2)}, u32[]{:S(2)}) collective-permute-start(bf16[384,512]{1,0:T(8,128)(2,1)S(1)} %get-tuple-element.15), channel_id=1, source_target_pairs={{0,1},{1,0},{2,3},{3,2},{4,5},{5,4},{6,7},{7,6},{8,9},{9,8},{10,11... | collective-permute-start | bytes 1179656 | tf_op jit(solution)/shard_map/ppermute | solution.py:83
  271.3 10.7 %collective-permute-start.28 = (bf16[256,512]{1,0:T(8,128)(2,1)}, bf16[256,512]{1,0:T(8,128)(2,1)S(1)}, u32[]{:S(2)}, u32[]{:S(2)}) collective-permute-start(bf16[256,512]{1,0:T(8,128)(2,1)} %collective-permute-done.27), channel_id=1, source_target_pairs={{0,16},{16,0},{1,17},{17,1},{2,18},{18,2},{3,19},{19,3},{4,20},{20... | collective-permute-start | bytes 786440 | tf_op jit(solution)/shard_map/ppermute | solution.py:47
  274.6 10.4 %collective-permute-start.31 = (bf16[256,512]{1,0:T(8,128)(2,1)}, bf16[256,512]{1,0:T(8,128)(2,1)S(1)}, u32[]{:S(2)}, u32[]{:S(2)}) collective-permute-start(bf16[256,512]{1,0:T(8,128)(2,1)} %collective-permute-done.29), channel_id=1, source_target_pairs={{0,4},{4,8},{8,12},{12,0},{1,5},{5,9},{9,13},{13,1},{2,6},{6,10},{... | collective-permute-start | bytes 786440 | tf_op jit(solution)/shard_map/ppermute | solution.py:45
  277.1 11.3 %collective-permute-start.30 = (bf16[256,512]{1,0:T(8,128)(2,1)}, bf16[256,512]{1,0:T(8,128)(2,1)S(1)}, u32[]{:S(2)}, u32[]{:S(2)}) collective-permute-start(bf16[256,512]{1,0:T(8,128)(2,1)} %collective-permute-done.29), channel_id=1, source_target_pairs={{0,16},{16,0},{1,17},{17,1},{2,18},{18,2},{3,19},{19,3},{4,20},{20... | collective-permute-start | bytes 786440 | tf_op jit(solution)/shard_map/ppermute | solution.py:47
  285.3 8.4 %collective-permute-start.47 = (bf16[384,512]{1,0:T(8,128)(2,1)S(1)}, bf16[384,512]{1,0:T(8,128)(2,1)S(1)}, u32[]{:S(2)}, u32[]{:S(2)}) collective-permute-start(bf16[384,512]{1,0:T(8,128)(2,1)S(1)} %get-tuple-element.16), channel_id=1, source_target_pairs={{0,1},{1,0},{2,3},{3,2},{4,5},{5,4},{6,7},{7,6},{8,9},{9,8},{10,11... | collective-permute-start | bytes 1179656 | tf_op jit(solution)/shard_map/ppermute | solution.py:83
  285.4 11.6 %collective-permute-start.46 = (bf16[384,512]{1,0:T(8,128)(2,1)S(1)}, bf16[384,512]{1,0:T(8,128)(2,1)S(1)}, u32[]{:S(2)}, u32[]{:S(2)}) collective-permute-start(bf16[384,512]{1,0:T(8,128)(2,1)S(1)} %add_convert_fusion.2), channel_id=1, source_target_pairs={{0,2},{1,3},{2,0},{3,1},{4,6},{5,7},{6,4},{7,5},{8,10},{9,11},{10,... | collective-permute-start | bytes 1179656 | tf_op jit(solution)/shard_map/ppermute | solution.py:86
  300.1 10.7 %collective-permute-start.49 = (bf16[384,512]{1,0:T(8,128)(2,1)S(1)}, bf16[384,512]{1,0:T(8,128)(2,1)S(1)}, u32[]{:S(2)}, u32[]{:S(2)}) collective-permute-start(bf16[384,512]{1,0:T(8,128)(2,1)S(1)} %get-tuple-element.24), channel_id=1, source_target_pairs={{0,2},{1,3},{2,0},{3,1},{4,6},{5,7},{6,4},{7,5},{8,10},{9,11},{10,... | collective-permute-start | bytes 1179656 | tf_op jit(solution)/shard_map/ppermute | solution.py:67
  301.4 14.9 %collective-permute-start.48 = (bf16[384,512]{1,0:T(8,128)(2,1)S(1)}, bf16[384,512]{1,0:T(8,128)(2,1)S(1)}, u32[]{:S(2)}, u32[]{:S(2)}) collective-permute-start(bf16[384,512]{1,0:T(8,128)(2,1)S(1)} %get-tuple-element.24), channel_id=1, source_target_pairs={{0,1},{1,0},{2,3},{3,2},{4,5},{5,4},{6,7},{7,6},{8,9},{9,8},{10,11... | collective-permute-start | bytes 1179656 | tf_op jit(solution)/shard_map/ppermute | solution.py:65
  344.1 11.4 %collective-permute-start.52 = (bf16[384,512]{1,0:T(8,128)(2,1)S(1)}, bf16[384,512]{1,0:T(8,128)(2,1)S(1)}, u32[]{:S(2)}, u32[]{:S(2)}) collective-permute-start(bf16[384,512]{1,0:T(8,128)(2,1)S(1)} %add_convert_fusion.1), channel_id=1, source_target_pairs={{0,2},{1,3},{2,0},{3,1},{4,6},{5,7},{6,4},{7,5},{8,10},{9,11},{10,... | collective-permute-start | bytes 1179656 | tf_op jit(solution)/shard_map/ppermute | solution.py:86
  (56 other events, 369.4 us)
